TPU v7x, 1024 devices: a whole 4x8x16 slice. The times are simulated.
1024 devices in a mesh: ep: 32 (over z, core), tp: 32 (over y, x).
Axes of the slice: x: 4, y: 8, z: 16, core: 2. Of those that a mesh axis runs over, the one named last changes fastest.
Arguments:
- tokens: bfloat16 [512, 4096], P('ep', 'tp'), may hold values from -40 to 40
- routes: int32 [512, 4], P('ep'), may hold values from 0 to 63, all different within a row; in each aligned block of 16 rows (0 to 15, 16 to 31, ...) at most 2 rows name the same one
- gates: float32 [512, 4], P('ep'), may hold values from 0.1 to 1
- pre_gain: bfloat16 [4096], P('tp'), may hold values from 0.099609375 to 1.8984375
- expert_gate: bfloat16 [64, 4096, 1024], P('ep', 'tp'), may hold values from -0.09375 to 0.09375
- expert_up: bfloat16 [64, 4096, 1024], P('ep', 'tp'), may hold values from -0.09375 to 0.09375
- expert_down: bfloat16 [64, 1024, 4096], P('ep', None, 'tp'), may hold values from -0.125 to 0.125
- shared_gate: bfloat16 [4096, 1024], P('tp'), may hold values from -0.09375 to 0.09375
- shared_up: bfloat16 [4096, 1024], P('tp'), may hold values from -0.09375 to 0.09375
- shared_down: bfloat16 [1024, 4096], P(None, 'tp'), may hold values from -0.125 to 0.125
- out_gain: bfloat16 [4096], P('tp'), may hold values from 0.099609375 to 1.8984375
Outputs:
- mixed: bfloat16 [512, 4096], P('ep', 'tp')
Inputs may be any that keep to these rules, and one draw needn't show every extreme that they name: `routes`: each row names 4 different experts, and expert e is held by index e // 2 of ep. Among the 16 rows of one index of ep no expert is named by more than 2 rows, and in every draw some expert is named by exactly 2 rows of some index.
All inputs are finite; a program needn't handle non-finite values.
Results may differ from a plain program's by a relative error of at most 0.012.
Values may be sent and summed in bfloat16 or wider, within the bound.
No kernel may reach another device: no remote copies, remote signals or barrier semaphores. Data moves between devices by JAX's collectives and lax.ppermute only.
A program may use at most 32 MiB of HBM per device.

v0:
```python
import jax
import jax.numpy as jnp
from jax import lax
from jax.sharding import PartitionSpec as P

D = 4096


def in_blocks(shard, dim, peers):
    before, after = (shard.shape[:dim], shard.shape[dim + 1 :])
    return jnp.moveaxis(shard.reshape(*before, peers, -1, *after), dim, 0)


def sent_and_summed(shard, axis, dim):
    peers = lax.axis_size(axis)
    tiles = lax.all_to_all(in_blocks(shard, dim, peers), axis, 0, 0, tiled=True)
    return jnp.sum(tiles.astype(jnp.float32), axis=0)


def side_by_side(arrays, axis, dim, along):
    widths = [a.shape[along] for a in arrays]
    both = jnp.concatenate(arrays, axis=along)
    filled = sent_and_summed(both, axis, dim)
    return tuple(jnp.split(filled, [sum(widths[:k]) for k in range(1, len(widths))], axis=along))


def rows_first(arrays, axis, dims):
    turned = [jnp.moveaxis(a, dim, 0) for a, dim in zip(arrays, dims)]
    both = jnp.concatenate([t.reshape(len(t), -1) for t in turned], axis=1)
    filled, at, outs = (lax.all_gather(both, axis, axis=0, tiled=True), 0, [])
    for t, dim in zip(turned, dims):
        section = filled[:, at : at + t[0].size].reshape(-1, *t.shape[1:])
        outs.append(jnp.moveaxis(section, 0, dim))
        at += t[0].size
    return tuple(outs)


def sent_to_all(shard, axis):
    peers = lax.axis_size(axis)
    return lax.all_to_all(
        jnp.broadcast_to(shard[None], (peers, *shard.shape)), axis, 0, 0, tiled=True
    )


def over_copies(shard, axis):
    return sent_to_all(shard, axis).sum(axis=0)


def normalize(values, gain, squares, width):
    scale = lax.rsqrt(squares[:, None] / width + 1e-06)
    return values * scale * gain.astype(jnp.float32)


def expert_apply(buffer, expert_gate, expert_up, expert_down, shared_gate_part, shared_up_part):
    gate_part = jnp.einsum(
        "secd,edf->secf", buffer, expert_gate, preferred_element_type=jnp.float32
    )
    up_part = jnp.einsum("secd,edf->secf", buffer, expert_up, preferred_element_type=jnp.float32)
    full_shape = gate_part.shape
    row_count = full_shape[0] * full_shape[1] * full_shape[2]
    gate_rows = gate_part.reshape(row_count, full_shape[3])
    up_rows = up_part.reshape(row_count, full_shape[3])
    gate_share, up_share, shared_gate_share, shared_up_share = side_by_side(
        (
            gate_rows.astype(jnp.bfloat16),
            up_rows.astype(jnp.bfloat16),
            shared_gate_part.astype(jnp.bfloat16),
            shared_up_part.astype(jnp.bfloat16),
        ),
        "tp",
        1,
        0,
    )
    hidden_share = (jax.nn.silu(gate_share) * up_share).astype(jnp.bfloat16)
    shared_share = (jax.nn.silu(shared_gate_share) * shared_up_share).astype(jnp.bfloat16)
    hidden_rows, shared_hidden = rows_first((hidden_share, shared_share), "tp", (1, 1))
    hidden = hidden_rows.reshape(full_shape)
    results = jnp.einsum(
        "secf,efd->secd", hidden, expert_down, preferred_element_type=jnp.float32
    ).astype(jnp.bfloat16)
    return (results, shared_hidden)


def on_device(
    tokens,
    routes,
    gates,
    pre_gain,
    expert_gate,
    expert_up,
    expert_down,
    shared_gate,
    shared_up,
    shared_down,
    out_gain,
):
    own_rows = tokens.astype(jnp.float32)
    in_squares = over_copies(jnp.sum(own_rows * own_rows, axis=1), "tp")
    normed = normalize(own_rows, pre_gain, in_squares, D).astype(jnp.bfloat16)
    shared_gate_part = jnp.dot(normed, shared_gate, preferred_element_type=jnp.float32)
    shared_up_part = jnp.dot(normed, shared_up, preferred_element_type=jnp.float32)
    tok_count = tokens.shape[0]
    top_count = routes.shape[1]
    groups = lax.axis_size("ep")
    local_experts = expert_gate.shape[0]
    experts_all = local_experts * groups
    capacity = max(2, 3 * tok_count * top_count // (2 * experts_all))
    places = jnp.arange(capacity, dtype=jnp.int32)
    zero_value = jnp.zeros((), jnp.float32)
    labels = jnp.arange(experts_all, dtype=jnp.int32)
    picked = routes[:, :, None] == labels[None, None, :]
    onehot = jnp.sum(picked.astype(jnp.int32), axis=1)
    dense_gate = jnp.sum(jnp.where(picked, gates[:, :, None], zero_value), axis=1)
    slot_index = jnp.cumsum(onehot, axis=0) - onehot
    select = (slot_index.T[:, None, :] == places[None, :, None]) & (onehot.T[:, None, :] > 0)
    outgoing = jnp.einsum(
        "ect,td->ecd", select.astype(jnp.bfloat16), normed, preferred_element_type=jnp.float32
    ).astype(jnp.bfloat16)
    outgoing = outgoing.reshape(groups, local_experts, capacity, normed.shape[1])
    received = lax.all_to_all(outgoing, "ep", split_axis=0, concat_axis=0, tiled=True)
    results, shared_hidden = expert_apply(
        received, expert_gate, expert_up, expert_down, shared_gate_part, shared_up_part
    )
    returned = lax.all_to_all(results, "ep", split_axis=0, concat_axis=0, tiled=True)
    weight = jnp.where(select, dense_gate.T[:, None, :], zero_value)
    returned_rows = returned.reshape(experts_all, capacity, normed.shape[1]).astype(jnp.float32)
    routed = jnp.einsum("ect,ecd->td", weight, returned_rows, precision=lax.Precision.HIGHEST)
    shared_out = jnp.dot(shared_hidden, shared_down, preferred_element_type=jnp.float32)
    combined = routed + shared_out
    out_squares = over_copies(jnp.sum(combined * combined, axis=1), "tp")
    return normalize(combined, out_gain, out_squares, D).astype(jnp.bfloat16)


def solution(mesh):
    in_specs = (
        P("ep", "tp"),
        P("ep", None),
        P("ep", None),
        P("tp"),
        P("ep", "tp", None),
        P("ep", "tp", None),
        P("ep", None, "tp"),
        P("tp", None),
        P("tp", None),
        P(None, "tp"),
        P("tp"),
    )
    out_specs = P("ep", "tp")
    return jax.shard_map(
        on_device, mesh=mesh, in_specs=in_specs, out_specs=out_specs, check_vma=False
    )
```

profile of v0, /device:TPU:1, one launch (start us, length us, event | category | flops | bytes accessed | tf_op | source)
XLA Modules:
  0.0 167.3 jit_solution(2424527635686730110)
XLA Ops:
  0.0 0.9 fusion.18
  0.9 0.6 broadcast_in_dim.32
  1.5 10.5 %all-to-all-start = ((f32[32,1,16]{2,1,0:T(1,128)}), f32[32,1,16]{2,1,0:T(1,128)S(1)}, u32[]{:S(2)}, u32[]{:S(2)}) async-start(f32[32,1,16]{2,1,0:T(1,128)} %broadcast_in_dim.32), calls=%async_computation | async-start | bytes 32768 | tf_op jit(solution)/shard_map/all_to_all | solution.py:40
  12.0 0.8 convert_reduce_fusion.1
  12.8 0.7 convert_element_type.64
  13.4 7.2 %all-to-all-done = f32[32,1,16]{2,1,0:T(1,128)S(1)} async-done(((f32[32,1,16]{2,1,0:T(1,128)}), f32[32,1,16]{2,1,0:T(1,128)S(1)}, u32[]{:S(2)}, u32[]{:S(2)}) %all-to-all-start) | async-done | bytes 2080 | tf_op jit(solution)/shard_map/all_to_all | solution.py:40
  20.7 0.9 convolution_convert_fusion.5
  21.6 0.6 copy.46
  22.2 20.9 %all-to-all-start.1 = ((bf16[32,2,2,128]{3,2,1,0:T(2,128)(2,1)}), bf16[32,2,2,128]{3,2,1,0:T(2,128)(2,1)S(1)}, u32[]{:S(2)}, u32[]{:S(2)}) async-start(bf16[32,2,2,128]{3,2,1,0:T(2,128)(2,1)} %copy.46), calls=%async_computation.1 | async-start | bytes 65536 | tf_op jit(solution)/shard_map/all_to_all | solution.py:120
  43.1 1.2 convolution_convert_fusion.3
  44.2 1.2 convolution_convert_fusion.4
  45.4 9.7 %all-to-all-done.1 = bf16[32,2,2,128]{3,2,1,0:T(2,128)(2,1)S(1)} async-done(((bf16[32,2,2,128]{3,2,1,0:T(2,128)(2,1)}), bf16[32,2,2,128]{3,2,1,0:T(2,128)(2,1)S(1)}, u32[]{:S(2)}, u32[]{:S(2)}) %all-to-all-start.1) | async-done | bytes 32800 | tf_op jit(solution)/shard_map/all_to_all | solution.py:120
  55.1 0.2 fusion
  55.3 0.3 copy.48
  55.7 0.2 fusion.1
  56.0 0.3 copy.50
  56.4 1.2 copy.51
  57.6 4.0 %all-to-all-start.2 = ((bf16[32,288,32]{1,2,0:T(8,128)(2,1)}), bf16[32,288,32]{1,2,0:T(8,128)(2,1)S(1)}, u32[]{:S(2)}, u32[]{:S(2)}) async-start(bf16[32,288,32]{1,2,0:T(8,128)(2,1)} %bitcast.12), calls=%async_computation.2 | async-start | bytes 1572864 | tf_op jit(solution)/shard_map/all_to_all | solution.py:16
  61.7 20.9 %all-to-all-done.2 = bf16[32,288,32]{1,2,0:T(8,128)(2,1)S(1)} async-done(((bf16[32,288,32]{1,2,0:T(8,128)(2,1)}), bf16[32,288,32]{1,2,0:T(8,128)(2,1)S(1)}, u32[]{:S(2)}, u32[]{:S(2)}) %all-to-all-start.2) | async-done | bytes 589856 | tf_op jit(solution)/shard_map/all_to_all | solution.py:16
  82.8 37.6 %all_gather.3 = bf16[1024,144]{1,0:T(8,128)(2,1)S(1)} all-gather(bf16[32,144]{1,0:T(8,128)(2,1)S(1)} %pad_maximum_fusion.1), channel_id=1, replica_groups=mesh['ep'=32,'tp'=32] {'tp'}, dimensions={0}, use_global_device_ids=true | all-gather | bytes 304128 | tf_op jit(solution)/shard_map/all_gather | solution.py:30
  120.5 0.1 copy.52
  120.8 0.7 copy-done.2
  121.5 0.2 fusion.2
  121.8 0.6 copy.54
  122.4 17.5 %all-to-all-start.3 = ((bf16[32,2,2,128]{3,2,1,0:T(2,128)(2,1)}), bf16[32,2,2,128]{3,2,1,0:T(2,128)(2,1)S(1)}, u32[]{:S(2)}, u32[]{:S(2)}) async-start(bf16[32,2,2,128]{3,2,1,0:T(2,128)(2,1)} %copy.54), calls=%async_computation.3 | async-start | bytes 65536 | tf_op jit(solution)/shard_map/all_to_all | solution.py:124
  139.9 0.2 fusion.7
  140.1 12.0 %all-to-all-done.3 = bf16[32,2,2,128]{3,2,1,0:T(2,128)(2,1)S(1)} async-done(((bf16[32,2,2,128]{3,2,1,0:T(2,128)(2,1)}), bf16[32,2,2,128]{3,2,1,0:T(2,128)(2,1)S(1)}, u32[]{:S(2)}, u32[]{:S(2)}) %all-to-all-start.3) | async-done | bytes 32800 | tf_op jit(solution)/shard_map/all_to_all | solution.py:124
  152.2 0.3 multiply_reduce_fusion
  152.5 0.6 broadcast_in_dim.33
  153.1 4.8 %all-to-all-start.4 = ((f32[32,1,16]{2,1,0:T(1,128)}), f32[32,1,16]{2,1,0:T(1,128)S(1)}, u32[]{:S(2)}, u32[]{:S(2)}) async-start(f32[32,1,16]{2,1,0:T(1,128)} %broadcast_in_dim.33), calls=%async_computation.4 | async-start | bytes 32768 | tf_op jit(solution)/shard_map/all_to_all | solution.py:40
  157.9 8.6 %all-to-all-done.4 = f32[32,1,16]{2,1,0:T(1,128)S(1)} async-done(((f32[32,1,16]{2,1,0:T(1,128)}), f32[32,1,16]{2,1,0:T(1,128)S(1)}, u32[]{:S(2)}, u32[]{:S(2)}) %all-to-all-start.4) | async-done | bytes 2080 | tf_op jit(solution)/shard_map/all_to_all | solution.py:40
  166.6 0.7 multiply_convert_fusion
  (32 shorter events, 0.9 us)
Async XLA Ops:
  0.0 55.1 %copy-start = (bf16[2,128,1024]{2,1,0:T(8,128)(2,1)S(1)}, bf16[2,128,1024]{2,1,0:T(8,128)(2,1)}, u32[]{:S(2)}) copy-start(bf16[2,128,1024]{2,1,0:T(8,128)(2,1)} %param.15) | copy-start | bytes 1572868
  1.5 19.1 %all-to-all-start = ((f32[32,1,16]{2,1,0:T(1,128)}), f32[32,1,16]{2,1,0:T(1,128)S(1)}, u32[]{:S(2)}, u32[]{:S(2)}) async-start(f32[32,1,16]{2,1,0:T(1,128)} %broadcast_in_dim.32), calls=%async_computation | async-start | bytes 32768 | tf_op jit(solution)/shard_map/all_to_all | solution.py:40
  22.2 32.9 %all-to-all-start.1 = ((bf16[32,2,2,128]{3,2,1,0:T(2,128)(2,1)}), bf16[32,2,2,128]{3,2,1,0:T(2,128)(2,1)S(1)}, u32[]{:S(2)}, u32[]{:S(2)}) async-start(bf16[32,2,2,128]{3,2,1,0:T(2,128)(2,1)} %copy.46), calls=%async_computation.1 | async-start | bytes 65536 | tf_op jit(solution)/shard_map/all_to_all | solution.py:120
  45.4 10.3 %copy-start.1 = (bf16[2,128,1024]{2,1,0:T(8,128)(2,1)S(1)}, bf16[2,128,1024]{2,1,0:T(8,128)(2,1)}, u32[]{:S(2)}) copy-start(bf16[2,128,1024]{2,1,0:T(8,128)(2,1)} %param.16) | copy-start | bytes 1572868
  57.6 4.1 %copy-start.4 = (s32[16,4]{0,1:T(4,128)S(1)}, s32[16,4]{0,1:T(4,128)}, u32[]{:S(2)}) copy-start(s32[16,4]{0,1:T(4,128)} %param.12) | copy-start | bytes 772
  57.6 4.1 %copy-start.5 = (f32[16,4]{0,1:T(4,128)S(1)}, f32[16,4]{0,1:T(4,128)}, u32[]{:S(2)}) copy-start(f32[16,4]{0,1:T(4,128)} %param.13) | copy-start | bytes 772
  57.6 25.1 %all-to-all-start.2 = ((bf16[32,288,32]{1,2,0:T(8,128)(2,1)}), bf16[32,288,32]{1,2,0:T(8,128)(2,1)S(1)}, u32[]{:S(2)}, u32[]{:S(2)}) async-start(bf16[32,288,32]{1,2,0:T(8,128)(2,1)} %bitcast.12), calls=%async_computation.2 | async-start | bytes 1572864 | tf_op jit(solution)/shard_map/all_to_all | solution.py:16
  120.5 1.0 copy-start.2
  120.7 19.2 %copy-start.3 = (bf16[1024,128]{1,0:T(8,128)(2,1)S(1)}, bf16[1024,128]{1,0:T(8,128)(2,1)}, u32[]{:S(2)}) copy-start(bf16[1024,128]{1,0:T(8,128)(2,1)} %param.20) | copy-start | bytes 786436
  121.5 36.4 %copy-start.6 = (bf16[128]{0:T(256)(128)(2,1)S(1)}, bf16[128]{0:T(256)(128)(2,1)}, u32[]{:S(2)}) copy-start(bf16[128]{0:T(256)(128)(2,1)} %param.21) | copy-start | bytes 772
  122.4 29.7 %all-to-all-start.3 = ((bf16[32,2,2,128]{3,2,1,0:T(2,128)(2,1)}), bf16[32,2,2,128]{3,2,1,0:T(2,128)(2,1)S(1)}, u32[]{:S(2)}, u32[]{:S(2)}) async-start(bf16[32,2,2,128]{3,2,1,0:T(2,128)(2,1)} %copy.54), calls=%async_computation.3 | async-start | bytes 65536 | tf_op jit(solution)/shard_map/all_to_all | solution.py:124
  153.1 13.4 %all-to-all-start.4 = ((f32[32,1,16]{2,1,0:T(1,128)}), f32[32,1,16]{2,1,0:T(1,128)S(1)}, u32[]{:S(2)}, u32[]{:S(2)}) async-start(f32[32,1,16]{2,1,0:T(1,128)} %broadcast_in_dim.33), calls=%async_computation.4 | async-start | bytes 32768 | tf_op jit(solution)/shard_map/all_to_all | solution.py:40
where the time goes:
time: 168 us; the launch traced here: 167 us
  waiting for transfers between devices  58.4 us (35%)
  starting transfers between devices  57.7 us (34%)
  blocking collectives  37.6 us (22%)
  local copies, waits for them, and re-layouts  5.44 us (3%)
  matrix products  4.43 us (3%)
  other arithmetic  3.47 us (2%)
    all_gather x1, blocking collectives, rows_first(): filled, at, outs = (lax.all_gather(both, axis, axis=0, tiled=True), 0, [])  37.6 us
    all_to_all x1, waiting for transfers between devices, sent_and_summed(): tiles = lax.all_to_all(in_blocks(shard, dim, peers), axis, 0, 0, tiled=True)  20.9 us
    all_to_all x1, starting transfers between devices, on_device(): lax.all_to_all(outgoing, 'ep', split_axis=0, concat_axis=0, tiled=True)  20.9 us
    all_to_all x1, starting transfers between devices, on_device(): lax.all_to_all(results, 'ep', split_axis=0, concat_axis=0, tiled=True)  17.5 us
    all_to_all x2, waiting for transfers between devices, sent_to_all(): lax.all_to_all(jnp.broadcast_to(shard[None], (peers, *shard.shape)), axis...  15.8 us
    all_to_all x2, starting transfers between devices, sent_to_all(): lax.all_to_all(jnp.broadcast_to(shard[None], (peers, *shard.shape)), axis...  15.3 us
    all_to_all x1, waiting for transfers between devices, on_device(): lax.all_to_all(results, 'ep', split_axis=0, concat_axis=0, tiled=True)  12 us
    all_to_all x1, waiting for transfers between devices, on_device(): lax.all_to_all(outgoing, 'ep', split_axis=0, concat_axis=0, tiled=True)  9.71 us
  transfers between devices with their start and end apart: 5, of which 5 were waited for; matrix products, arithmetic and copies ran while one was open for 2% of the time, Pallas kernels for 0%

commit v1 on v0

v1 whole, which is shorter than its diff:
```python
import jax
import jax.numpy as jnp
from jax import lax
from jax.experimental import pallas as pl
from jax.experimental.pallas import tpu as pltpu
from jax.sharding import PartitionSpec as P

D = 4096
EPS = 1e-06
PEERS = 32
LANES = 128
ROWS = 128
GROUPS = 4
BLOCK = 80
HID = 40
F32 = jnp.float32
BF16 = jnp.bfloat16
I32 = jnp.int32


def iota(shape, dim):
    return lax.broadcasted_iota(I32, shape, dim)


def dot(a, b):
    return jnp.dot(a, b, preferred_element_type=F32)


def slot_choice(routes_t):
    tok = routes_t.shape[1]
    slot = iota((ROWS, tok), 0)
    expert = slot >> 1
    named = jnp.zeros((ROWS, tok), F32)
    for k in range(4):
        named = named + jnp.where(routes_t[k : k + 1, :] == expert, 1.0, 0.0)
    earlier = jnp.where(iota((tok, tok), 0) < iota((tok, tok), 1), 1.0, 0.0)
    before = dot(named.astype(BF16), earlier.astype(BF16))
    place = (slot & 1).astype(F32)
    return jnp.where((named > 0.5) & (before == place), 1.0, 0.0)


def dispatch_kernel(tokens_ref, routes_ref, out_ref):
    choice = slot_choice(routes_ref[...])
    out_ref[...] = dot(choice.astype(BF16), tokens_ref[...]).astype(BF16)


def row_of(col, lanes_from):
    n = col.shape[0]
    hit = iota((n, LANES), 1) == iota((n, LANES), 0) + lanes_from
    return jnp.sum(jnp.where(hit, col, 0.0), axis=0, keepdims=True)


def col_of(row, n, lanes_from):
    hit = iota((n, LANES), 1) == iota((n, LANES), 0) + lanes_from
    return jnp.sum(jnp.where(hit, row, 0.0), axis=1, keepdims=True)


def project_kernel(recv_ref, tokens_ref, gain_ref, wg_ref, wu_ref, sg_ref, su_ref, out_ref):
    gain = gain_ref[...].astype(F32)
    to_row = iota((ROWS, ROWS), 0)
    from_row = ((to_row & 31) << 2) + (to_row >> 5)
    swap = jnp.where(iota((ROWS, ROWS), 1) == from_row, 1.0, 0.0).astype(BF16)
    rows = dot(swap, recv_ref[...])
    row_sq = jnp.sum(rows * rows, axis=1, keepdims=True)
    scaled = (rows * gain).astype(BF16)
    tr = iota((32, 16), 0)
    take = jnp.where(iota((32, 16), 1) == ((tr >> 3) << 2) + (tr & 3), 1.0, 0.0).astype(BF16)
    toks = dot(take, tokens_ref[...])
    tok_sq = jnp.sum(toks * toks, axis=1, keepdims=True)
    toks_scaled = (toks * gain).astype(BF16)
    shared_g = dot(toks_scaled, sg_ref[...])
    shared_u = dot(toks_scaled, su_ref[...])
    shared = jnp.where((iota((32, 1024), 0) & 7) < 4, shared_g, shared_u)
    sub = iota((8, LANES), 0)
    for e in range(2):
        x = scaled[64 * e : 64 * e + 64]
        g = dot(x, wg_ref[e]).astype(BF16)
        u = dot(x, wu_ref[e]).astype(BF16)
        for c in range(2):
            r = 2 * e + c
            sq = row_of(row_sq[32 * r : 32 * r + 32], 0) + row_of(tok_sq[8 * r : 8 * r + 8], 64)
            hi = sq.astype(BF16).astype(F32)
            lo = sq - hi
            sq8 = jnp.where(sub == 0, hi, jnp.where(sub == 1, lo, 0.0))
            for l in range(8):
                p = 8 * r + l
                cols = slice(128 * l, 128 * l + 128)
                out_ref[p, 0:32, :] = g[32 * c : 32 * c + 32, cols]
                out_ref[p, 32:64, :] = u[32 * c : 32 * c + 32, cols]
                tail = jnp.concatenate([shared[8 * r : 8 * r + 8, cols], sq8], axis=0)
                out_ref[p, 64:80, :] = tail.astype(BF16)


def silu(v):
    return v / (1.0 + jnp.exp(-v))


def hidden_kernel(recv_ref, out_ref):
    total = jnp.sum(recv_ref[...].astype(F32), axis=0)
    sq = total[72:73] + total[73:74]
    row_scale = lax.rsqrt(col_of(sq, 32, 0) / D + EPS)
    hid = silu(total[0:32] * row_scale) * (total[32:64] * row_scale)
    tok_scale = lax.rsqrt(col_of(sq, 8, 64) / D + EPS)
    both = total[64:72] * tok_scale
    up = pltpu.roll(both, 4, 0)
    shared = jnp.where(iota((8, LANES), 0) < 4, silu(both) * up, 0.0)
    piece = jnp.concatenate([hid, shared], axis=0).astype(BF16)
    out_ref[...] = jnp.broadcast_to(piece[None], out_ref.shape)


def down_kernel(recv_ref, wd_ref, out_ref):
    parts = []
    for e in range(2):
        lhs = jnp.concatenate(
            [
                jnp.concatenate([recv_ref[8 * (2 * e + c) + l, 0:32, :] for l in range(8)], axis=1)
                for c in range(2)
            ],
            axis=0,
        )
        parts.append(dot(lhs, wd_ref[e]).astype(BF16))
    rows = jnp.concatenate(parts, axis=0)
    to_row = iota((ROWS, ROWS), 0)
    from_row = ((to_row & 3) << 5) + (to_row >> 2)
    swap = jnp.where(iota((ROWS, ROWS), 1) == from_row, 1.0, 0.0).astype(BF16)
    out_ref[...] = dot(swap, rows).astype(BF16)


def shared_kernel(recv_ref, sd_ref, routes_ref, gates_ref, shared_ref, weight_ref):
    lhs = jnp.concatenate(
        [
            jnp.concatenate([recv_ref[8 * r + l, 32:40, :] for l in range(8)], axis=1)
            for r in range(4)
        ],
        axis=0,
    )
    full = dot(lhs, sd_ref[...])
    shared_ref[...] = jnp.concatenate([full[8 * r : 8 * r + 4] for r in range(4)], axis=0)
    routes_t = routes_ref[...]
    gates_t = gates_ref[...]
    choice = slot_choice(routes_t)
    expert = iota(choice.shape, 0) >> 1
    gate = jnp.zeros(choice.shape, F32)
    for k in range(4):
        gate = gate + jnp.where(routes_t[k : k + 1, :] == expert, gates_t[k : k + 1, :], 0.0)
    weight_ref[...] = jnp.transpose(choice * gate)


def combine_kernel(recv_ref, weight_ref, shared_ref, out_ref, sq_ref):
    routed = jnp.dot(
        weight_ref[...],
        recv_ref[...].astype(F32),
        precision=lax.Precision.HIGHEST,
        preferred_element_type=F32,
    )
    combined = routed + shared_ref[...]
    out_ref[...] = combined
    sq = row_of(jnp.sum(combined * combined, axis=1, keepdims=True), 0)
    sq_ref[...] = jnp.broadcast_to(sq[None], sq_ref.shape)


def final_kernel(sq_ref, combined_ref, gain_ref, out_ref):
    sq = jnp.sum(sq_ref[...], axis=0)
    scale = lax.rsqrt(col_of(sq, 16, 0) / D + EPS)
    out_ref[...] = (combined_ref[...] * scale * gain_ref[...].astype(F32)).astype(BF16)


def call(kernel, out, *args):
    return pl.pallas_call(kernel, out_shape=out)(*args)


def shape(dims, dtype):
    return jax.ShapeDtypeStruct(dims, dtype)


def swapped(x, axis):
    return lax.all_to_all(x, axis, 0, 0, tiled=True)


def on_device(
    tokens,
    routes,
    gates,
    pre_gain,
    expert_gate,
    expert_up,
    expert_down,
    shared_gate,
    shared_up,
    shared_down,
    out_gain,
):
    routes_t = routes.T
    gates_t = gates.T
    outgoing = call(dispatch_kernel, shape((ROWS, LANES), BF16), tokens, routes_t)
    received = swapped(outgoing.reshape(PEERS, GROUPS, LANES), "ep").reshape(ROWS, LANES)
    partial = call(
        project_kernel,
        shape((PEERS, BLOCK, LANES), BF16),
        received,
        tokens,
        pre_gain.reshape(1, LANES),
        expert_gate,
        expert_up,
        shared_gate,
        shared_up,
    )
    summands = swapped(partial, "tp")
    piece = call(hidden_kernel, shape((PEERS, HID, LANES), BF16), summands)
    hidden = swapped(piece, "tp")
    results = call(down_kernel, shape((ROWS, LANES), BF16), hidden, expert_down)
    returned = swapped(results.reshape(PEERS, GROUPS, LANES), "ep").reshape(ROWS, LANES)
    shared_out, weight = call(
        shared_kernel,
        (shape((16, LANES), F32), shape((16, ROWS), F32)),
        hidden,
        shared_down,
        routes_t,
        gates_t,
    )
    combined, squares = call(
        combine_kernel,
        (shape((16, LANES), F32), shape((PEERS, 1, LANES), F32)),
        returned,
        weight,
        shared_out,
    )
    squares = swapped(squares, "tp")
    return call(
        final_kernel,
        shape((16, LANES), BF16),
        squares,
        combined,
        out_gain.reshape(1, LANES),
    )


def solution(mesh):
    in_specs = (
        P("ep", "tp"),
        P("ep", None),
        P("ep", None),
        P("tp"),
        P("ep", "tp", None),
        P("ep", "tp", None),
        P("ep", None, "tp"),
        P("tp", None),
        P("tp", None),
        P(None, "tp"),
        P("tp"),
    )
    return jax.shard_map(
        on_device, mesh=mesh, in_specs=in_specs, out_specs=P("ep", "tp"), check_vma=False
    )
```

time: 168 us -> 123 us (0.73)
  blocking collectives: 37.6 us -> 90.3 us
  starting transfers between devices: 57.7 us -> 7.94 us
  waiting for transfers between devices: 58.4 us -> 10.3 us
  Pallas kernels: 0 us -> 13.4 us
  local copies, waits for them, and re-layouts: 5.44 us -> 0.61 us
  matrix products: 4.43 us -> 0 us
  other arithmetic: 3.47 us -> 0 us
    all_to_all x0 -> x4, blocking collectives: none -> 90.3 us  [swapped(): return lax.all_to_all(x, axis, 0, 0, tiled=True)]
    all_to_all x5 -> x1, starting transfers between devices: 57.7 us -> 7.94 us  [swapped(): return lax.all_to_all(x, axis, 0, 0, tiled=True)]
    all_to_all x5 -> x1, waiting for transfers between devices: 58.4 us -> 10.3 us  [swapped(): return lax.all_to_all(x, axis, 0, 0, tiled=True)]
    all_gather x1 -> x0, blocking collectives: 37.6 us -> none  [rows_first(): filled, at, outs = (lax.all_gather(both, axis, axis=0, tiled=True), 0, [])]
    pallas_call x0 -> x7, Pallas kernels: none -> 13.4 us  [call(): return pl.pallas_call(kernel, out_shape=out)(*args)]
    dot_general x8 -> x0, matrix products: 4.43 us -> none  [the longest x1 1.17 us: on_device(): jnp.dot(normed, shared_gate, preferred_element_type=jnp.float32)]
    reduce_sum x6 -> x0, other arithmetic: 1.93 us -> none  [the longest x1 0.86 us: on_device(): in_squares = over_copies(jnp.sum(own_rows * own_rows, axis=1), 'tp')]
  transfers between devices with their start and end apart: 5 -> 1, of which waited for: 5 -> 1; matrix products, arithmetic and copies ran while one was open for 2% -> 0% of each run, Pallas kernels for 0% -> 2%
where the time goes in v1:
time: 123 us
  blocking collectives  90.3 us (73%)
  Pallas kernels  13.4 us (11%)
  waiting for transfers between devices  10.3 us (8%)
  starting transfers between devices  7.94 us (6%)
    all_to_all x4, blocking collectives, swapped(): return lax.all_to_all(x, axis, 0, 0, tiled=True)  90.3 us
    pallas_call x7, Pallas kernels, call(): return pl.pallas_call(kernel, out_shape=out)(*args)  13.4 us
    all_to_all x1, waiting for transfers between devices, swapped(): return lax.all_to_all(x, axis, 0, 0, tiled=True)  10.3 us
    all_to_all x1, starting transfers between devices, swapped(): return lax.all_to_all(x, axis, 0, 0, tiled=True)  7.94 us
  transfers between devices with their start and end apart: 1, of which 1 were waited for; matrix products, arithmetic and copies ran while one was open for 0% of the time, Pallas kernels for 2%

profile of v1, /device:TPU:1, one launch (start us, length us, event | category | flops | bytes accessed | tf_op | source)
XLA Modules:
  0.0 122.6 jit_solution(13189334453379061351)
XLA Ops:
  0.0 1.6 %shard_map.109 = bf16[128,128]{1,0:T(8,128)(2,1)} custom-call(bf16[16,128]{1,0:T(8,128)(2,1)} %tokens_ref.3, s32[4,16]{1,0:T(4,128)} %bitcast.12), custom_call_target="tpu_custom_call" | custom-call | tf_op jit(solution)/shard_map/pallas_call | solution.py:169
  1.6 32.6 %all_to_all.25 = bf16[32,4,128]{2,1,0:T(4,128)(2,1)} all-to-all(bf16[32,4,128]{2,1,0:T(4,128)(2,1)} %bitcast.11), channel_id=1, replica_groups=mesh['ep'=32,'tp'=32] {'ep'}, dimensions={0} | all-to-all | bytes 65536 | tf_op jit(solution)/shard_map/all_to_all | solution.py:177
  34.1 2.7 %shard_map.110 = bf16[32,80,128]{2,1,0:T(8,128)(2,1)} custom-call(bf16[128,128]{1,0:T(8,128)(2,1)} %bitcast.8, bf16[16,128]{1,0:T(8,128)(2,1)} %tokens_ref.3, bf16[1,128]{1,0:T(2,128)(2,1)} %bitcast.15, bf16[2,128,1024]{2,1,0:T(8,128)(2,1)} %wg_ref.1, bf16[2,128,1024]{2,1,0:T(8,128)(2,1)} %wu_ref.1, bf16[128,1024]{1,0:T(8,128)(2,1)} %sg_ref.1, ...), custom_call_target="tpu_custom_call" | custom-call | tf_op jit(solution)/shard_map/pallas_call | solution.py:169
  36.9 28.0 %all_to_all.26.recv_ref = bf16[32,80,128]{2,1,0:T(8,128)(2,1)} all-to-all(bf16[32,80,128]{2,1,0:T(8,128)(2,1)} %shard_map.110), channel_id=1, replica_groups=mesh['ep'=32,'tp'=32] {'tp'}, dimensions={0} | all-to-all | bytes 1310720 | tf_op jit(solution)/shard_map/all_to_all | solution.py:177
  64.8 2.0 %shard_map.111 = bf16[32,40,128]{2,1,0:T(8,128)(2,1)} custom-call(bf16[32,80,128]{2,1,0:T(8,128)(2,1)} %all_to_all.26.recv_ref), custom_call_target="tpu_custom_call" | custom-call | tf_op jit(solution)/shard_map/pallas_call | solution.py:169
  66.8 16.9 %all_to_all.27.recv_ref = bf16[32,40,128]{2,1,0:T(8,128)(2,1)} all-to-all(bf16[32,40,128]{2,1,0:T(8,128)(2,1)} %shard_map.111), channel_id=1, replica_groups=mesh['ep'=32,'tp'=32] {'tp'}, dimensions={0} | all-to-all | bytes 655360 | tf_op jit(solution)/shard_map/all_to_all | solution.py:177
  83.7 2.1 %shard_map.112 = bf16[128,128]{1,0:T(8,128)(2,1)} custom-call(bf16[32,40,128]{2,1,0:T(8,128)(2,1)} %all_to_all.27.recv_ref, bf16[2,1024,128]{2,1,0:T(8,128)(2,1)} %wd_ref.1), custom_call_target="tpu_custom_call" | custom-call | tf_op jit(solution)/shard_map/pallas_call | solution.py:169
  85.8 7.9 %all-to-all-start.3 = ((bf16[32,4,128]{2,1,0:T(4,128)(2,1)}), bf16[32,4,128]{2,1,0:T(4,128)(2,1)S(1)}, u32[]{:S(2)}, u32[]{:S(2)}) async-start(bf16[32,4,128]{2,1,0:T(4,128)(2,1)} %bitcast.9), calls=%async_computation.3 | async-start | bytes 65536 | tf_op jit(solution)/shard_map/all_to_all | solution.py:177
  93.7 1.9 %shard_map.113 = (f32[16,128]{1,0:T(8,128)}, f32[16,128]{1,0:T(8,128)}) custom-call(bf16[32,40,128]{2,1,0:T(8,128)(2,1)} %all_to_all.27.recv_ref, bf16[1024,128]{1,0:T(8,128)(2,1)} %sd_ref.1, s32[4,16]{1,0:T(4,128)} %bitcast.13, f32[4,16]{1,0:T(4,128)} %bitcast.14), custom_call_target="tpu_custom_call" | custom-call | tf_op jit(solution)/shard_map/pallas_call | solution.py:169
  95.7 10.3 %all-to-all-done.3 = bf16[32,4,128]{2,1,0:T(4,128)(2,1)S(1)} async-done(((bf16[32,4,128]{2,1,0:T(4,128)(2,1)}), bf16[32,4,128]{2,1,0:T(4,128)(2,1)S(1)}, u32[]{:S(2)}, u32[]{:S(2)}) %all-to-all-start.3) | async-done | bytes 32800 | tf_op jit(solution)/shard_map/all_to_all | solution.py:177
  106.0 0.0 copy-start
  106.0 0.6 copy-done
  106.6 1.6 %shard_map.114 = (f32[16,128]{1,0:T(8,128)}, f32[32,1,128]{2,1,0:T(1,128)}) custom-call(bf16[128,128]{1,0:T(8,128)(2,1)} %bitcast.10, f32[16,128]{1,0:T(8,128)} %get-tuple-element.9.weight_ref, f32[16,128]{1,0:T(8,128)} %get-tuple-element.10.shared_ref), custom_call_target="tpu_custom_call" | custom-call | tf_op jit(solution)/shard_map/pallas_call | solution.py:169
  108.2 12.9 %all_to_all.28.sq_ref = f32[32,1,128]{2,1,0:T(1,128)} all-to-all(f32[32,1,128]{2,1,0:T(1,128)} %get-tuple-element.11), channel_id=1, replica_groups=mesh['ep'=32,'tp'=32] {'tp'}, dimensions={0} | all-to-all | bytes 32768 | tf_op jit(solution)/shard_map/all_to_all | solution.py:177
  121.2 1.5 %shard_map.115 = bf16[16,128]{1,0:T(8,128)(2,1)} custom-call(f32[32,1,128]{2,1,0:T(1,128)} %all_to_all.28.sq_ref, f32[16,128]{1,0:T(8,128)} %get-tuple-element.12.combined_ref, bf16[1,128]{1,0:T(2,128)(2,1)} %bitcast.16), custom_call_target="tpu_custom_call" | custom-call | tf_op jit(solution)/shard_map/pallas_call | solution.py:169
Async XLA Ops:
  85.8 20.2 %all-to-all-start.3 = ((bf16[32,4,128]{2,1,0:T(4,128)(2,1)}), bf16[32,4,128]{2,1,0:T(4,128)(2,1)S(1)}, u32[]{:S(2)}, u32[]{:S(2)}) async-start(bf16[32,4,128]{2,1,0:T(4,128)(2,1)} %bitcast.9), calls=%async_computation.3 | async-start | bytes 65536 | tf_op jit(solution)/shard_map/all_to_all | solution.py:177
  106.0 0.6 copy-start

commit v2 on v1

--- a/solution.py
+++ b/solution.py
@@ -39,9 +39,35 @@
     return jnp.where((named > 0.5) & (before == place), 1.0, 0.0)
 
 
-def dispatch_kernel(tokens_ref, routes_ref, out_ref):
+def loads(pairs, sems):
+    copies = [pltpu.make_async_copy(src, dst, sems.at[i]) for i, (src, dst) in enumerate(pairs)]
+    for c in copies:
+        c.start()
+    return copies
+
+
+def dispatch_kernel(
+    tokens_in, routes_in, gain_in, wg_in, wu_in, sg_in, su_in,
+    out_ref, tokens_ref, routes_ref, gain_ref, wg_ref, wu_ref, sg_ref, su_ref, sems,
+):
+    copies = loads(
+        (
+            (routes_in, routes_ref),
+            (tokens_in, tokens_ref),
+            (gain_in, gain_ref),
+            (wg_in, wg_ref),
+            (wu_in, wu_ref),
+            (sg_in, sg_ref),
+            (su_in, su_ref),
+        ),
+        sems,
+    )
+    copies[0].wait()
     choice = slot_choice(routes_ref[...])
+    copies[1].wait()
     out_ref[...] = dot(choice.astype(BF16), tokens_ref[...]).astype(BF16)
+    for c in copies[2:]:
+        c.wait()
 
 
 def row_of(col, lanes_from):
@@ -55,7 +81,13 @@
     return jnp.sum(jnp.where(hit, row, 0.0), axis=1, keepdims=True)
 
 
-def project_kernel(recv_ref, tokens_ref, gain_ref, wg_ref, wu_ref, sg_ref, su_ref, out_ref):
+def project_kernel(
+    recv_ref, tokens_ref, gain_ref, wg_ref, wu_ref, sg_ref, su_ref, wd_in, sd_in, gates_in, last_in,
+    out_ref, wd_ref, sd_ref, gates_ref, last_ref, sems,
+):
+    copies = loads(
+        ((wd_in, wd_ref), (sd_in, sd_ref), (gates_in, gates_ref), (last_in, last_ref)), sems
+    )
     gain = gain_ref[...].astype(F32)
     to_row = iota((ROWS, ROWS), 0)
     from_row = ((to_row & 31) << 2) + (to_row >> 5)
@@ -89,6 +121,8 @@
                 out_ref[p, 32:64, :] = u[32 * c : 32 * c + 32, cols]
                 tail = jnp.concatenate([shared[8 * r : 8 * r + 8, cols], sq8], axis=0)
                 out_ref[p, 64:80, :] = tail.astype(BF16)
+    for copy in copies:
+        copy.wait()
 
 
 def silu(v):
@@ -108,7 +142,9 @@
     out_ref[...] = jnp.broadcast_to(piece[None], out_ref.shape)
 
 
-def down_kernel(recv_ref, wd_ref, out_ref):
+def down_kernel(
+    recv_ref, wd_ref, sd_ref, routes_ref, gates_ref, out_ref, shared_ref, weight_ref
+):
     parts = []
     for e in range(2):
         lhs = jnp.concatenate(
@@ -124,9 +160,6 @@
     from_row = ((to_row & 3) << 5) + (to_row >> 2)
     swap = jnp.where(iota((ROWS, ROWS), 1) == from_row, 1.0, 0.0).astype(BF16)
     out_ref[...] = dot(swap, rows).astype(BF16)
-
-
-def shared_kernel(recv_ref, sd_ref, routes_ref, gates_ref, shared_ref, weight_ref):
     lhs = jnp.concatenate(
         [
             jnp.concatenate([recv_ref[8 * r + l, 32:40, :] for l in range(8)], axis=1)
@@ -165,12 +198,23 @@
     out_ref[...] = (combined_ref[...] * scale * gain_ref[...].astype(F32)).astype(BF16)
 
 
-def call(kernel, out, *args):
-    return pl.pallas_call(kernel, out_shape=out)(*args)
-
-
-def shape(dims, dtype):
-    return jax.ShapeDtypeStruct(dims, dtype)
+def call(kernel, out, fast, slow=()):
+    return pl.pallas_call(
+        kernel,
+        out_shape=out,
+        in_specs=[pl.BlockSpec(memory_space=pltpu.VMEM)] * len(fast)
+        + [pl.BlockSpec(memory_space=pltpu.HBM)] * len(slow),
+        scratch_shapes=[pltpu.SemaphoreType.DMA((len(slow),))] if slow else [],
+        compiler_params=pltpu.CompilerParams(vmem_limit_bytes=16 << 20),
+    )(*[pltpu.with_memory_space_constraint(a, pltpu.VMEM) for a in fast], *[pltpu.with_memory_space_constraint(a, pltpu.HBM) for a in slow])
+
+
+def fast(dims, dtype):
+    return pltpu.VMEM(dims, dtype)
+
+
+def like(a):
+    return pltpu.VMEM(a.shape, a.dtype)
 
 
 def swapped(x, axis):
@@ -190,48 +234,45 @@
     shared_down,
     out_gain,
 ):
-    routes_t = routes.T
-    gates_t = gates.T
-    outgoing = call(dispatch_kernel, shape((ROWS, LANES), BF16), tokens, routes_t)
-    received = swapped(outgoing.reshape(PEERS, GROUPS, LANES), "ep").reshape(ROWS, LANES)
-    partial = call(
-        project_kernel,
-        shape((PEERS, BLOCK, LANES), BF16),
-        received,
+    first = (
         tokens,
+        routes.T,
         pre_gain.reshape(1, LANES),
         expert_gate,
         expert_up,
         shared_gate,
         shared_up,
     )
+    outgoing, tokens, routes, gain, *weights = call(
+        dispatch_kernel, (fast((ROWS, LANES), BF16), *[like(a) for a in first]), (), first
+    )
+    received = swapped(outgoing.reshape(PEERS, GROUPS, LANES), "ep").reshape(ROWS, LANES)
+    later = (expert_down, shared_down, gates.T, out_gain.reshape(1, LANES))
+    partial, expert_down, shared_down, gates, out_gain = call(
+        project_kernel,
+        (fast((PEERS, BLOCK, LANES), BF16), *[like(a) for a in later]),
+        (received, tokens, gain, *weights),
+        later,
+    )
     summands = swapped(partial, "tp")
-    piece = call(hidden_kernel, shape((PEERS, HID, LANES), BF16), summands)
+    piece = call(hidden_kernel, fast((PEERS, HID, LANES), BF16), (summands,))
     hidden = swapped(piece, "tp")
-    results = call(down_kernel, shape((ROWS, LANES), BF16), hidden, expert_down)
+    results, shared_out, weight = call(
+        down_kernel,
+        (fast((ROWS, LANES), BF16), fast((16, LANES), F32), fast((16, ROWS), F32)),
+        (hidden, expert_down, shared_down, routes, gates),
+    )
     returned = swapped(results.reshape(PEERS, GROUPS, LANES), "ep").reshape(ROWS, LANES)
-    shared_out, weight = call(
-        shared_kernel,
-        (shape((16, LANES), F32), shape((16, ROWS), F32)),
-        hidden,
-        shared_down,
-        routes_t,
-        gates_t,
-    )
     combined, squares = call(
         combine_kernel,
-        (shape((16, LANES), F32), shape((PEERS, 1, LANES), F32)),
-        returned,
-        weight,
-        shared_out,
+        (fast((16, LANES), F32), fast((PEERS, 1, LANES), F32)),
+        (returned, weight, shared_out),
     )
     squares = swapped(squares, "tp")
     return call(
         final_kernel,
-        shape((16, LANES), BF16),
-        squares,
-        combined,
-        out_gain.reshape(1, LANES),
+        jax.ShapeDtypeStruct((16, LANES), BF16),
+        (squares, combined, out_gain),
     )
 
 

time: 123 us -> 112 us (0.911)
  blocking collectives: 90.3 us -> 108 us
  waiting for transfers between devices: 10.3 us -> 0 us
  Pallas kernels: 13.4 us -> 4.18 us
  starting transfers between devices: 7.94 us -> 0 us
    all_to_all x4 -> x5, blocking collectives: 90.3 us -> 108 us  [swapped(): return lax.all_to_all(x, axis, 0, 0, tiled=True)]
    all_to_all x1 -> x0, waiting for transfers between devices: 10.3 us -> none  [swapped(): return lax.all_to_all(x, axis, 0, 0, tiled=True)]
    pallas_call x7 -> x6, Pallas kernels: 13.4 us -> 4.18 us  [call(): pl.pallas_call(kernel, out_shape=out, in_specs=[pl.BlockSpec(memory_space...]
    all_to_all x1 -> x0, starting transfers between devices: 7.94 us -> none  [swapped(): return lax.all_to_all(x, axis, 0, 0, tiled=True)]
  transfers between devices with their start and end apart: 1 -> 0, of which waited for: 1 -> 0; matrix products, arithmetic and copies ran while one was open for 0% -> 0% of each run, Pallas kernels for 2% -> 0%
where the time goes in v2:
time: 112 us
  blocking collectives  108 us (96%)
  Pallas kernels  4.18 us (4%)
    all_to_all x5, blocking collectives, swapped(): return lax.all_to_all(x, axis, 0, 0, tiled=True)  108 us
    pallas_call x6, Pallas kernels, call(): pl.pallas_call(kernel, out_shape=out, in_specs=[pl.BlockSpec(memory_space...  4.18 us

profile of v2, /device:TPU:1, one launch (start us, length us, event | category | flops | bytes accessed | tf_op | source)
XLA Modules:
  0.0 112.1 jit_solution(14138526665836851803)
XLA Ops:
  0.0 1.5 %shard_map.109 = (bf16[128,128]{1,0:T(8,128)(2,1)S(1)}, bf16[16,128]{1,0:T(8,128)(2,1)S(1)}, s32[4,16]{1,0:T(4,128)S(1)}, bf16[1,128]{1,0:T(2,128)(2,1)S(1)}, bf...) custom-call(bf16[16,128]{1,0:T(8,128)(2,1)} %tokens_in.1, ...), custom_call_target="tpu_custom_call" | custom-call | tf_op jit(solution)/shard_map/pallas_call | solution.py:202
  1.5 32.3 %all_to_all.25 = bf16[32,4,128]{2,1,0:T(4,128)(2,1)S(1)} all-to-all(bf16[32,4,128]{2,1,0:T(4,128)(2,1)S(1)} %bitcast.10), channel_id=1, replica_groups=mesh['ep'=32,'tp'=32] {'ep'}, dimensions={0} | all-to-all | bytes 65536 | tf_op jit(solution)/shard_map/all_to_all | solution.py:221
  33.7 1.2 %shard_map.110 = (bf16[32,80,128]{2,1,0:T(8,128)(2,1)S(1)}, bf16[2,1024,128]{2,1,0:T(8,128)(2,1)S(1)}, bf16[1024,128]{1,0:T(8,128)(2,1)S(1)}, f32[4,16]{1,0:T(4,128)S(1)}, bf16[1,128]{1,0:T(2,128)(2,1)S(1)}) custom-call(bf16[128,128]{1,0:T(8,128)(2,1)S(1)} %bitcast.8, bf16[16,128]{1,0:T(8,128)(2,1)S(1)} %get-tuple-element.24.tokens_ref, ...), custom_call_target="tpu_custom_call" | custom-call | tf_op jit(solution)/shard_map/pallas_call | solution.py:202
  34.9 27.7 %all_to_all.26.recv_ref = bf16[32,80,128]{2,1,0:T(8,128)(2,1)S(1)} all-to-all(bf16[32,80,128]{2,1,0:T(8,128)(2,1)S(1)} %get-tuple-element.30), channel_id=1, replica_groups=mesh['ep'=32,'tp'=32] {'tp'}, dimensions={0} | all-to-all | bytes 1310720 | tf_op jit(solution)/shard_map/all_to_all | solution.py:221
  62.6 0.2 shard_map.111
  62.8 16.6 %all_to_all.27.recv_ref = bf16[32,40,128]{2,1,0:T(8,128)(2,1)S(1)} all-to-all(bf16[32,40,128]{2,1,0:T(8,128)(2,1)S(1)} %shard_map.111), channel_id=1, replica_groups=mesh['ep'=32,'tp'=32] {'tp'}, dimensions={0} | all-to-all | bytes 655360 | tf_op jit(solution)/shard_map/all_to_all | solution.py:221
  79.3 0.4 shard_map.112
  79.7 19.4 %all_to_all.28 = bf16[32,4,128]{2,1,0:T(4,128)(2,1)S(1)} all-to-all(bf16[32,4,128]{2,1,0:T(4,128)(2,1)S(1)} %bitcast.11), channel_id=1, replica_groups=mesh['ep'=32,'tp'=32] {'ep'}, dimensions={0} | all-to-all | bytes 65536 | tf_op jit(solution)/shard_map/all_to_all | solution.py:221
  99.1 0.3 shard_map.113
  99.4 12.0 %all_to_all.29.sq_ref = f32[32,1,128]{2,1,0:T(1,128)S(1)} all-to-all(f32[32,1,128]{2,1,0:T(1,128)S(1)} %get-tuple-element.38), channel_id=1, replica_groups=mesh['ep'=32,'tp'=32] {'tp'}, dimensions={0} | all-to-all | bytes 32768 | tf_op jit(solution)/shard_map/all_to_all | solution.py:221
  111.4 0.7 shard_map.114

commit v3 on v2

--- a/solution.py
+++ b/solution.py
@@ -10,9 +10,8 @@
 PEERS = 32
 LANES = 128
 ROWS = 128
-GROUPS = 4
-BLOCK = 80
-HID = 40
+BLOCK = 74
+HID = 36
 F32 = jnp.float32
 BF16 = jnp.bfloat16
 I32 = jnp.int32
@@ -103,24 +102,28 @@
     shared_g = dot(toks_scaled, sg_ref[...])
     shared_u = dot(toks_scaled, su_ref[...])
     shared = jnp.where((iota((32, 1024), 0) & 7) < 4, shared_g, shared_u)
-    sub = iota((8, LANES), 0)
+    sub = iota((2, LANES), 0)
     for e in range(2):
         x = scaled[64 * e : 64 * e + 64]
-        g = dot(x, wg_ref[e]).astype(BF16)
-        u = dot(x, wu_ref[e]).astype(BF16)
+        g = dot(x, wg_ref[e])
+        u = dot(x, wu_ref[e])
         for c in range(2):
             r = 2 * e + c
             sq = row_of(row_sq[32 * r : 32 * r + 32], 0) + row_of(tok_sq[8 * r : 8 * r + 8], 64)
             hi = sq.astype(BF16).astype(F32)
-            lo = sq - hi
-            sq8 = jnp.where(sub == 0, hi, jnp.where(sub == 1, lo, 0.0))
-            for l in range(8):
-                p = 8 * r + l
-                cols = slice(128 * l, 128 * l + 128)
-                out_ref[p, 0:32, :] = g[32 * c : 32 * c + 32, cols]
-                out_ref[p, 32:64, :] = u[32 * c : 32 * c + 32, cols]
-                tail = jnp.concatenate([shared[8 * r : 8 * r + 8, cols], sq8], axis=0)
-                out_ref[p, 64:80, :] = tail.astype(BF16)
+            sq2 = jnp.where(sub == 0, hi, sq - hi)
+            for half in range(2):
+                blocks = []
+                for l in range(4 * half, 4 * half + 4):
+                    cols = slice(128 * l, 128 * l + 128)
+                    blocks += [
+                        g[32 * c : 32 * c + 32, cols],
+                        u[32 * c : 32 * c + 32, cols],
+                        shared[8 * r : 8 * r + 8, cols],
+                        sq2,
+                    ]
+                at = (2 * r + half) * 4 * BLOCK
+                out_ref[at : at + 4 * BLOCK, :] = jnp.concatenate(blocks, axis=0).astype(BF16)
     for copy in copies:
         copy.wait()
 
@@ -130,45 +133,46 @@
 
 
 def hidden_kernel(recv_ref, out_ref):
-    total = jnp.sum(recv_ref[...].astype(F32), axis=0)
+    four = recv_ref[0 : 4 * BLOCK, :].astype(F32)
+    for q in range(1, PEERS // 4):
+        four = four + recv_ref[4 * BLOCK * q : 4 * BLOCK * q + 4 * BLOCK, :].astype(F32)
+    total = four[0:BLOCK]
+    for i in range(1, 4):
+        total = total + four[BLOCK * i : BLOCK * i + BLOCK]
     sq = total[72:73] + total[73:74]
     row_scale = lax.rsqrt(col_of(sq, 32, 0) / D + EPS)
     hid = silu(total[0:32] * row_scale) * (total[32:64] * row_scale)
     tok_scale = lax.rsqrt(col_of(sq, 8, 64) / D + EPS)
     both = total[64:72] * tok_scale
     up = pltpu.roll(both, 4, 0)
-    shared = jnp.where(iota((8, LANES), 0) < 4, silu(both) * up, 0.0)
-    piece = jnp.concatenate([hid, shared], axis=0).astype(BF16)
-    out_ref[...] = jnp.broadcast_to(piece[None], out_ref.shape)
+    shared = (silu(both) * up)[0:4]
+    piece = jnp.concatenate([hid, shared, hid, shared], axis=0).astype(BF16)
+    for q in range(PEERS // 2):
+        out_ref[2 * HID * q : 2 * HID * q + 2 * HID, :] = piece
 
 
 def down_kernel(
     recv_ref, wd_ref, sd_ref, routes_ref, gates_ref, out_ref, shared_ref, weight_ref
 ):
+    pairs = [recv_ref[2 * HID * q : 2 * HID * q + 2 * HID, :] for q in range(PEERS // 2)]
+
+    def wide(at, n, r):
+        return jnp.concatenate(
+            [pairs[4 * r + l // 2][HID * (l % 2) + at : HID * (l % 2) + at + n] for l in range(8)],
+            axis=1,
+        )
+
     parts = []
     for e in range(2):
-        lhs = jnp.concatenate(
-            [
-                jnp.concatenate([recv_ref[8 * (2 * e + c) + l, 0:32, :] for l in range(8)], axis=1)
-                for c in range(2)
-            ],
-            axis=0,
-        )
+        lhs = jnp.concatenate([wide(0, 32, 2 * e), wide(0, 32, 2 * e + 1)], axis=0)
         parts.append(dot(lhs, wd_ref[e]).astype(BF16))
     rows = jnp.concatenate(parts, axis=0)
     to_row = iota((ROWS, ROWS), 0)
     from_row = ((to_row & 3) << 5) + (to_row >> 2)
     swap = jnp.where(iota((ROWS, ROWS), 1) == from_row, 1.0, 0.0).astype(BF16)
     out_ref[...] = dot(swap, rows).astype(BF16)
-    lhs = jnp.concatenate(
-        [
-            jnp.concatenate([recv_ref[8 * r + l, 32:40, :] for l in range(8)], axis=1)
-            for r in range(4)
-        ],
-        axis=0,
-    )
-    full = dot(lhs, sd_ref[...])
-    shared_ref[...] = jnp.concatenate([full[8 * r : 8 * r + 4] for r in range(4)], axis=0)
+    lhs = jnp.concatenate([wide(32, 4, r) for r in range(4)], axis=0)
+    shared_ref[...] = dot(lhs, sd_ref[...])
     routes_t = routes_ref[...]
     gates_t = gates_ref[...]
     choice = slot_choice(routes_t)
@@ -217,8 +221,9 @@
     return pltpu.VMEM(a.shape, a.dtype)
 
 
-def swapped(x, axis):
-    return lax.all_to_all(x, axis, 0, 0, tiled=True)
+def swapped(x, axis, tile):
+    tiles = x.reshape(-1, tile, LANES)
+    return lax.all_to_all(tiles, axis, 0, 0, tiled=True).reshape(x.shape)
 
 
 def on_device(
@@ -246,29 +251,29 @@
     outgoing, tokens, routes, gain, *weights = call(
         dispatch_kernel, (fast((ROWS, LANES), BF16), *[like(a) for a in first]), (), first
     )
-    received = swapped(outgoing.reshape(PEERS, GROUPS, LANES), "ep").reshape(ROWS, LANES)
+    received = swapped(outgoing, "ep", 4)
     later = (expert_down, shared_down, gates.T, out_gain.reshape(1, LANES))
     partial, expert_down, shared_down, gates, out_gain = call(
         project_kernel,
-        (fast((PEERS, BLOCK, LANES), BF16), *[like(a) for a in later]),
+        (fast((PEERS * BLOCK, LANES), BF16), *[like(a) for a in later]),
         (received, tokens, gain, *weights),
         later,
     )
-    summands = swapped(partial, "tp")
-    piece = call(hidden_kernel, fast((PEERS, HID, LANES), BF16), (summands,))
-    hidden = swapped(piece, "tp")
+    summands = swapped(partial, "tp", 2)
+    piece = call(hidden_kernel, fast((PEERS * HID, LANES), BF16), (summands,))
+    hidden = swapped(piece, "tp", 4)
     results, shared_out, weight = call(
         down_kernel,
         (fast((ROWS, LANES), BF16), fast((16, LANES), F32), fast((16, ROWS), F32)),
         (hidden, expert_down, shared_down, routes, gates),
     )
-    returned = swapped(results.reshape(PEERS, GROUPS, LANES), "ep").reshape(ROWS, LANES)
+    returned = swapped(results, "ep", 4)
     combined, squares = call(
         combine_kernel,
         (fast((16, LANES), F32), fast((PEERS, 1, LANES), F32)),
         (returned, weight, shared_out),
     )
-    squares = swapped(squares, "tp")
+    squares = swapped(squares, "tp", 1)
     return call(
         final_kernel,
         jax.ShapeDtypeStruct((16, LANES), BF16),

time: 112 us -> 111 us (level)
  blocking collectives: 108 us -> 106 us
    all_to_all x5, blocking collectives: 108 us -> 106 us  [swapped(): return lax.all_to_all(tiles, axis, 0, 0, tiled=True).reshape(x.shape)]
where the time goes in v3:
time: 111 us; the launch traced here: 110 us
  blocking collectives  106 us (95%)
  Pallas kernels  4.09 us (4%)
    all_to_all x5, blocking collectives, swapped(): return lax.all_to_all(tiles, axis, 0, 0, tiled=True).reshape(x.shape)  106 us
    pallas_call x6, Pallas kernels, call(): pl.pallas_call(kernel, out_shape=out, in_specs=[pl.BlockSpec(memory_space...  4.09 us

profile of v3, /device:TPU:1, one launch (start us, length us, event | category | flops | bytes accessed | tf_op | source)
XLA Modules:
  0.0 110.3 jit_solution(15783635551520462)
XLA Ops:
  0.0 1.5 %shard_map.109 = (bf16[128,128]{1,0:T(8,128)(2,1)S(1)}, bf16[16,128]{1,0:T(8,128)(2,1)S(1)}, s32[4,16]{1,0:T(4,128)S(1)}, bf16[1,128]{1,0:T(2,128)(2,1)S(1)}, bf...) custom-call(bf16[16,128]{1,0:T(8,128)(2,1)} %tokens_in.1, ...), custom_call_target="tpu_custom_call" | custom-call | tf_op jit(solution)/shard_map/pallas_call | solution.py:206
  1.5 32.3 %all_to_all.25 = bf16[32,4,128]{2,1,0:T(4,128)(2,1)S(1)} all-to-all(bf16[32,4,128]{2,1,0:T(4,128)(2,1)S(1)} %bitcast.18), channel_id=1, replica_groups=mesh['ep'=32,'tp'=32] {'ep'}, dimensions={0} | all-to-all | bytes 65536 | tf_op jit(solution)/shard_map/all_to_all | solution.py:226
  33.7 1.1 %shard_map.110 = (bf16[2368,128]{1,0:T(8,128)(2,1)S(1)}, bf16[2,1024,128]{2,1,0:T(8,128)(2,1)S(1)}, bf16[1024,128]{1,0:T(8,128)(2,1)S(1)}, f32[4,16]{1,0:T(4,128)S(1)}, bf16[1,128]{1,0:T(2,128)(2,1)S(1)}) custom-call(bf16[128,128]{1,0:T(8,128)(2,1)S(1)} %bitcast.16, bf16[16,128]{1,0:T(8,128)(2,1)S(1)} %get-tuple-element.24.tokens_ref, ...), custom_call_target="tpu_custom_call" | custom-call | tf_op jit(solution)/shard_map/pallas_call | solution.py:206
  34.9 26.5 %all_to_all.26 = bf16[1184,2,128]{2,1,0:T(2,128)(2,1)S(1)} all-to-all(bf16[1184,2,128]{2,1,0:T(2,128)(2,1)S(1)} %bitcast.15), channel_id=1, replica_groups=mesh['ep'=32,'tp'=32] {'tp'}, dimensions={0} | all-to-all | bytes 1212416 | tf_op jit(solution)/shard_map/all_to_all | solution.py:226
  61.4 0.1 shard_map.111
  61.5 16.9 %all_to_all.27 = bf16[288,4,128]{2,1,0:T(4,128)(2,1)S(1)} all-to-all(bf16[288,4,128]{2,1,0:T(4,128)(2,1)S(1)} %bitcast.13), channel_id=1, replica_groups=mesh['ep'=32,'tp'=32] {'tp'}, dimensions={0} | all-to-all | bytes 589824 | tf_op jit(solution)/shard_map/all_to_all | solution.py:226
  78.5 0.4 shard_map.112
  78.9 18.4 %all_to_all.28 = bf16[32,4,128]{2,1,0:T(4,128)(2,1)S(1)} all-to-all(bf16[32,4,128]{2,1,0:T(4,128)(2,1)S(1)} %bitcast.19), channel_id=1, replica_groups=mesh['ep'=32,'tp'=32] {'ep'}, dimensions={0} | all-to-all | bytes 65536 | tf_op jit(solution)/shard_map/all_to_all | solution.py:226
  97.3 0.3 shard_map.113
  97.5 12.1 %all_to_all.29.sq_ref = f32[32,1,128]{2,1,0:T(1,128)S(1)} all-to-all(f32[32,1,128]{2,1,0:T(1,128)S(1)} %get-tuple-element.38), channel_id=1, replica_groups=mesh['ep'=32,'tp'=32] {'tp'}, dimensions={0} | all-to-all | bytes 32768 | tf_op jit(solution)/shard_map/all_to_all | solution.py:226
  109.6 0.7 shard_map.114

commit v4 on v3

--- a/solution.py
+++ b/solution.py
@@ -12,6 +12,7 @@
 ROWS = 128
 BLOCK = 74
 HID = 36
+WORK = 4 * 10**9
 F32 = jnp.float32
 BF16 = jnp.bfloat16
 I32 = jnp.int32
@@ -46,18 +47,16 @@
 
 
 def dispatch_kernel(
-    tokens_in, routes_in, gain_in, wg_in, wu_in, sg_in, su_in,
-    out_ref, tokens_ref, routes_ref, gain_ref, wg_ref, wu_ref, sg_ref, su_ref, sems,
+    routes_in, tokens_in, gates_in, gain_in, last_in,
+    out_ref, routes_ref, tokens_ref, gates_ref, gain_ref, last_ref, sems,
 ):
     copies = loads(
         (
             (routes_in, routes_ref),
             (tokens_in, tokens_ref),
+            (gates_in, gates_ref),
             (gain_in, gain_ref),
-            (wg_in, wg_ref),
-            (wu_in, wu_ref),
-            (sg_in, sg_ref),
-            (su_in, su_ref),
+            (last_in, last_ref),
         ),
         sems,
     )
@@ -80,13 +79,7 @@
     return jnp.sum(jnp.where(hit, row, 0.0), axis=1, keepdims=True)
 
 
-def project_kernel(
-    recv_ref, tokens_ref, gain_ref, wg_ref, wu_ref, sg_ref, su_ref, wd_in, sd_in, gates_in, last_in,
-    out_ref, wd_ref, sd_ref, gates_ref, last_ref, sems,
-):
-    copies = loads(
-        ((wd_in, wd_ref), (sd_in, sd_ref), (gates_in, gates_ref), (last_in, last_ref)), sems
-    )
+def project_kernel(recv_ref, tokens_ref, gain_ref, wg_ref, wu_ref, sg_ref, su_ref, out_ref):
     gain = gain_ref[...].astype(F32)
     to_row = iota((ROWS, ROWS), 0)
     from_row = ((to_row & 31) << 2) + (to_row >> 5)
@@ -124,8 +117,6 @@
                     ]
                 at = (2 * r + half) * 4 * BLOCK
                 out_ref[at : at + 4 * BLOCK, :] = jnp.concatenate(blocks, axis=0).astype(BF16)
-    for copy in copies:
-        copy.wait()
 
 
 def silu(v):
@@ -210,6 +201,7 @@
         + [pl.BlockSpec(memory_space=pltpu.HBM)] * len(slow),
         scratch_shapes=[pltpu.SemaphoreType.DMA((len(slow),))] if slow else [],
         compiler_params=pltpu.CompilerParams(vmem_limit_bytes=16 << 20),
+        cost_estimate=pl.CostEstimate(flops=WORK, bytes_accessed=1 << 16, transcendentals=0),
     )(*[pltpu.with_memory_space_constraint(a, pltpu.VMEM) for a in fast], *[pltpu.with_memory_space_constraint(a, pltpu.HBM) for a in slow])
 
 
@@ -240,24 +232,19 @@
     out_gain,
 ):
     first = (
+        routes.T,
         tokens,
-        routes.T,
+        gates.T,
         pre_gain.reshape(1, LANES),
-        expert_gate,
-        expert_up,
-        shared_gate,
-        shared_up,
-    )
-    outgoing, tokens, routes, gain, *weights = call(
+        out_gain.reshape(1, LANES),
+    )
+    outgoing, routes, tokens, gates, gain, out_gain = call(
         dispatch_kernel, (fast((ROWS, LANES), BF16), *[like(a) for a in first]), (), first
     )
     received = swapped(outgoing, "ep", 4)
-    later = (expert_down, shared_down, gates.T, out_gain.reshape(1, LANES))
-    partial, expert_down, shared_down, gates, out_gain = call(
-        project_kernel,
-        (fast((PEERS * BLOCK, LANES), BF16), *[like(a) for a in later]),
-        (received, tokens, gain, *weights),
-        later,
+    weights = (expert_gate, expert_up, shared_gate, shared_up)
+    partial = call(
+        project_kernel, fast((PEERS * BLOCK, LANES), BF16), (received, tokens, gain, *weights)
     )
     summands = swapped(partial, "tp", 2)
     piece = call(hidden_kernel, fast((PEERS * HID, LANES), BF16), (summands,))

time: 111 us -> 110 us (level)
  no operation moved by 1% of the time
where the time goes in v4:
time: 110 us
  blocking collectives  106 us (96%)
  Pallas kernels  3.12 us (3%)
    all_to_all x5, blocking collectives, swapped(): return lax.all_to_all(tiles, axis, 0, 0, tiled=True).reshape(x.shape)  106 us
    pallas_call x6, Pallas kernels, call(): pl.pallas_call(kernel, out_shape=out, in_specs=[pl.BlockSpec(memory_space...  3.12 us

profile of v4, /device:TPU:1, one launch (start us, length us, event | category | flops | bytes accessed | tf_op | source)
XLA Modules:
  0.0 109.5 jit_solution(15959228292948336471)
XLA Ops:
  0.0 0.0 copy-start
  0.0 0.0 copy-start.1
  0.0 0.0 copy-start.3
  0.0 0.0 copy-start.4
  0.0 1.1 %shard_map.109 = (bf16[128,128]{1,0:T(8,128)(2,1)S(1)}, s32[4,16]{1,0:T(4,128)S(1)}, bf16[16,128]{1,0:T(8,128)(2,1)S(1)}, f32[4,16]{1,0:T(4,128)S(1)}, bf16[1,12...) custom-call(s32[4,16]{1,0:T(4,128)} %bitcast.20, bf16[16,128]{1,0:T(8,128)(2,1)} %tokens_in.1, f32[4,16]{1,0:T(4,128)} %bitcast.21, ...), custom_call_target="tpu_custom_call" | custom-call | flops 4000000000 | bytes 65536 | tf_op jit(solution)/shard_map/pallas_call | solution.py:197
  1.2 32.3 %all_to_all.25 = bf16[32,4,128]{2,1,0:T(4,128)(2,1)S(1)} all-to-all(bf16[32,4,128]{2,1,0:T(4,128)(2,1)S(1)} %bitcast.16), channel_id=1, replica_groups=mesh['ep'=32,'tp'=32] {'ep'}, dimensions={0} | all-to-all | bytes 65536 | tf_op jit(solution)/shard_map/all_to_all | solution.py:218
  33.4 0.0 copy-done
  33.4 0.0 copy-done.1
  33.4 0.0 copy-done.3
  33.4 0.0 copy-done.4
  33.4 0.5 shard_map.110
  33.9 26.5 %all_to_all.26 = bf16[1184,2,128]{2,1,0:T(2,128)(2,1)S(1)} all-to-all(bf16[1184,2,128]{2,1,0:T(2,128)(2,1)S(1)} %bitcast.12), channel_id=1, replica_groups=mesh['ep'=32,'tp'=32] {'tp'}, dimensions={0} | all-to-all | bytes 1212416 | tf_op jit(solution)/shard_map/all_to_all | solution.py:218
  60.5 0.0 copy-start.5
  60.5 0.1 shard_map.111
  60.6 0.0 copy-start.2
  60.6 17.1 %all_to_all.27 = bf16[288,4,128]{2,1,0:T(4,128)(2,1)S(1)} all-to-all(bf16[288,4,128]{2,1,0:T(4,128)(2,1)S(1)} %bitcast.15), channel_id=1, replica_groups=mesh['ep'=32,'tp'=32] {'tp'}, dimensions={0} | all-to-all | bytes 589824 | tf_op jit(solution)/shard_map/all_to_all | solution.py:218
  77.7 0.0 copy-done.5
  77.7 0.0 copy-done.2
  77.7 0.4 shard_map.112
  78.1 18.4 %all_to_all.28 = bf16[32,4,128]{2,1,0:T(4,128)(2,1)S(1)} all-to-all(bf16[32,4,128]{2,1,0:T(4,128)(2,1)S(1)} %bitcast.17), channel_id=1, replica_groups=mesh['ep'=32,'tp'=32] {'ep'}, dimensions={0} | all-to-all | bytes 65536 | tf_op jit(solution)/shard_map/all_to_all | solution.py:218
  96.5 0.3 shard_map.113
  96.8 12.1 %all_to_all.29.sq_ref = f32[32,1,128]{2,1,0:T(1,128)S(1)} all-to-all(f32[32,1,128]{2,1,0:T(1,128)S(1)} %get-tuple-element.24), channel_id=1, replica_groups=mesh['ep'=32,'tp'=32] {'tp'}, dimensions={0} | all-to-all | bytes 32768 | tf_op jit(solution)/shard_map/all_to_all | solution.py:218
  108.8 0.7 shard_map.114
Async XLA Ops:
  0.0 33.4 %copy-start = (bf16[2,128,1024]{2,1,0:T(8,128)(2,1)S(1)}, bf16[2,128,1024]{2,1,0:T(8,128)(2,1)}, u32[]{:S(2)}) copy-start(bf16[2,128,1024]{2,1,0:T(8,128)(2,1)} %wg_ref.1) | copy-start | bytes 1572868
  0.0 33.4 %copy-start.1 = (bf16[2,128,1024]{2,1,0:T(8,128)(2,1)S(1)}, bf16[2,128,1024]{2,1,0:T(8,128)(2,1)}, u32[]{:S(2)}) copy-start(bf16[2,128,1024]{2,1,0:T(8,128)(2,1)} %wu_ref.1) | copy-start | bytes 1572868
  0.0 33.4 %copy-start.3 = (bf16[128,1024]{1,0:T(8,128)(2,1)S(1)}, bf16[128,1024]{1,0:T(8,128)(2,1)}, u32[]{:S(2)}) copy-start(bf16[128,1024]{1,0:T(8,128)(2,1)} %sg_ref.1) | copy-start | bytes 786436
  0.0 33.4 %copy-start.4 = (bf16[128,1024]{1,0:T(8,128)(2,1)S(1)}, bf16[128,1024]{1,0:T(8,128)(2,1)}, u32[]{:S(2)}) copy-start(bf16[128,1024]{1,0:T(8,128)(2,1)} %su_ref.1) | copy-start | bytes 786436
  60.5 17.2 %copy-start.5 = (bf16[1024,128]{1,0:T(8,128)(2,1)S(1)}, bf16[1024,128]{1,0:T(8,128)(2,1)}, u32[]{:S(2)}) copy-start(bf16[1024,128]{1,0:T(8,128)(2,1)} %sd_ref.1) | copy-start | bytes 786436
  60.6 17.1 %copy-start.2 = (bf16[2,1024,128]{2,1,0:T(8,128)(2,1)S(1)}, bf16[2,1024,128]{2,1,0:T(8,128)(2,1)}, u32[]{:S(2)}) copy-start(bf16[2,1024,128]{2,1,0:T(8,128)(2,1)} %wd_ref.1) | copy-start | bytes 1572868

commit v5 on v4

--- a/solution.py
+++ b/solution.py
@@ -3,11 +3,12 @@
 from jax import lax
 from jax.experimental import pallas as pl
 from jax.experimental.pallas import tpu as pltpu
-from jax.sharding import PartitionSpec as P
+from jax.sharding import Mesh, PartitionSpec as P
 
 D = 4096
 EPS = 1e-06
 PEERS = 32
+TP = ("y", "x")
 LANES = 128
 ROWS = 128
 BLOCK = 74
@@ -119,14 +120,20 @@
                 out_ref[at : at + 4 * BLOCK, :] = jnp.concatenate(blocks, axis=0).astype(BF16)
 
 
+def quarter_kernel(recv_ref, out_ref):
+    n = out_ref.shape[0]
+    total = recv_ref[0:n, :].astype(F32)
+    for i in range(1, 4):
+        total = total + recv_ref[n * i : n * i + n, :].astype(F32)
+    out_ref[...] = total.astype(BF16)
+
+
 def silu(v):
     return v / (1.0 + jnp.exp(-v))
 
 
 def hidden_kernel(recv_ref, out_ref):
-    four = recv_ref[0 : 4 * BLOCK, :].astype(F32)
-    for q in range(1, PEERS // 4):
-        four = four + recv_ref[4 * BLOCK * q : 4 * BLOCK * q + 4 * BLOCK, :].astype(F32)
+    four = recv_ref[0 : 4 * BLOCK, :].astype(F32) + recv_ref[4 * BLOCK :, :].astype(F32)
     total = four[0:BLOCK]
     for i in range(1, 4):
         total = total + four[BLOCK * i : BLOCK * i + BLOCK]
@@ -148,10 +155,8 @@
     pairs = [recv_ref[2 * HID * q : 2 * HID * q + 2 * HID, :] for q in range(PEERS // 2)]
 
     def wide(at, n, r):
-        return jnp.concatenate(
-            [pairs[4 * r + l // 2][HID * (l % 2) + at : HID * (l % 2) + at + n] for l in range(8)],
-            axis=1,
-        )
+        start = HID * (r % 2) + at
+        return jnp.concatenate([pairs[2 * l + r // 2][start : start + n] for l in range(8)], axis=1)
 
     parts = []
     for e in range(2):
@@ -246,9 +251,11 @@
     partial = call(
         project_kernel, fast((PEERS * BLOCK, LANES), BF16), (received, tokens, gain, *weights)
     )
-    summands = swapped(partial, "tp", 2)
+    over_x = swapped(partial, "x", 2)
+    quarter = call(quarter_kernel, fast((8 * BLOCK, LANES), BF16), (over_x,))
+    summands = swapped(quarter, "y", 2)
     piece = call(hidden_kernel, fast((PEERS * HID, LANES), BF16), (summands,))
-    hidden = swapped(piece, "tp", 4)
+    hidden = swapped(piece, TP, 4)
     results, shared_out, weight = call(
         down_kernel,
         (fast((ROWS, LANES), BF16), fast((16, LANES), F32), fast((16, ROWS), F32)),
@@ -260,7 +267,7 @@
         (fast((16, LANES), F32), fast((PEERS, 1, LANES), F32)),
         (returned, weight, shared_out),
     )
-    squares = swapped(squares, "tp", 1)
+    squares = swapped(squares, TP, 1)
     return call(
         final_kernel,
         jax.ShapeDtypeStruct((16, LANES), BF16),
@@ -269,19 +276,20 @@
 
 
 def solution(mesh):
+    mesh = Mesh(mesh.devices.reshape(-1, 8, 4), ("ep", "y", "x"))
     in_specs = (
-        P("ep", "tp"),
+        P("ep", TP),
         P("ep", None),
         P("ep", None),
-        P("tp"),
-        P("ep", "tp", None),
-        P("ep", "tp", None),
-        P("ep", None, "tp"),
-        P("tp", None),
-        P("tp", None),
-        P(None, "tp"),
-        P("tp"),
+        P(TP),
+        P("ep", TP, None),
+        P("ep", TP, None),
+        P("ep", None, TP),
+        P(TP, None),
+        P(TP, None),
+        P(None, TP),
+        P(TP),
     )
     return jax.shard_map(
-        on_device, mesh=mesh, in_specs=in_specs, out_specs=P("ep", "tp"), check_vma=False
-    )
+        on_device, mesh=mesh, in_specs=in_specs, out_specs=P("ep", TP), check_vma=False
+    )

time: 110 us -> 109 us (level)
    all_to_all x5 -> x6, blocking collectives: 106 us -> 105 us  [swapped(): return lax.all_to_all(tiles, axis, 0, 0, tiled=True).reshape(x.shape)]
    pallas_call x6 -> x7, Pallas kernels: 3.12 us -> 3.19 us  [call(): pl.pallas_call(kernel, out_shape=out, in_specs=[pl.BlockSpec(memory_space...]
where the time goes in v5:
time: 109 us
  blocking collectives  105 us (96%)
  Pallas kernels  3.19 us (3%)
    all_to_all x6, blocking collectives, swapped(): return lax.all_to_all(tiles, axis, 0, 0, tiled=True).reshape(x.shape)  105 us
    pallas_call x7, Pallas kernels, call(): pl.pallas_call(kernel, out_shape=out, in_specs=[pl.BlockSpec(memory_space...  3.19 us

profile of v5, /device:TPU:1, one launch (start us, length us, event | category | flops | bytes accessed | tf_op | source)
XLA Modules:
  0.0 108.7 jit_solution(18410908808199246948)
XLA Ops:
  0.0 0.0 copy-start
  0.0 0.0 copy-start.1
  0.0 0.0 copy-start.3
  0.0 0.0 copy-start.4
  0.0 1.1 %shard_map.109 = (bf16[128,128]{1,0:T(8,128)(2,1)S(1)}, s32[4,16]{1,0:T(4,128)S(1)}, bf16[16,128]{1,0:T(8,128)(2,1)S(1)}, f32[4,16]{1,0:T(4,128)S(1)}, bf16[1,12...) custom-call(s32[4,16]{1,0:T(4,128)} %bitcast.24, bf16[16,128]{1,0:T(8,128)(2,1)} %tokens_in.1, f32[4,16]{1,0:T(4,128)} %bitcast.25, ...), custom_call_target="tpu_custom_call" | custom-call | flops 4000000000 | bytes 65536 | tf_op jit(solution)/shard_map/pallas_call | solution.py:202
  1.2 32.3 %all_to_all.30 = bf16[32,4,128]{2,1,0:T(4,128)(2,1)S(1)} all-to-all(bf16[32,4,128]{2,1,0:T(4,128)(2,1)S(1)} %bitcast.20), channel_id=1, replica_groups=mesh['ep'=32,'y'=8,'x'=4] {'ep'}, dimensions={0} | all-to-all | bytes 65536 | tf_op jit(solution)/shard_map/all_to_all | solution.py:223
  33.4 0.0 copy-done
  33.4 0.0 copy-done.1
  33.4 0.0 copy-done.3
  33.4 0.0 copy-done.4
  33.4 0.5 shard_map.110
  33.9 12.8 %all_to_all.31 = bf16[1184,2,128]{2,1,0:T(2,128)(2,1)S(1)} all-to-all(bf16[1184,2,128]{2,1,0:T(2,128)(2,1)S(1)} %bitcast.14), channel_id=1, replica_groups=mesh['ep'=32,'y'=8,'x'=4] {'x'}, dimensions={0} | all-to-all | bytes 1212416 | tf_op jit(solution)/shard_map/all_to_all | solution.py:223
  46.8 0.1 shard_map.111
  46.9 14.9 %all_to_all.32 = bf16[296,2,128]{2,1,0:T(2,128)(2,1)S(1)} all-to-all(bf16[296,2,128]{2,1,0:T(2,128)(2,1)S(1)} %bitcast.18), channel_id=1, replica_groups=mesh['ep'=32,'y'=8,'x'=4] {'y'}, dimensions={0} | all-to-all | bytes 303104 | tf_op jit(solution)/shard_map/all_to_all | solution.py:223
  61.7 0.0 copy-start.5
  61.7 0.1 shard_map.112
  61.9 0.0 copy-start.2
  61.9 14.0 %all_to_all.33 = bf16[288,4,128]{2,1,0:T(4,128)(2,1)S(1)} all-to-all(bf16[288,4,128]{2,1,0:T(4,128)(2,1)S(1)} %bitcast.17), channel_id=1, replica_groups=mesh['ep'=32,'y'=8,'x'=4] {'y','x'}, dimensions={0} | all-to-all | bytes 589824 | tf_op jit(solution)/shard_map/all_to_all | solution.py:223
  75.9 0.0 copy-done.5
  75.9 0.0 copy-done.2
  75.9 0.4 shard_map.113
  76.3 19.7 %all_to_all.34 = bf16[32,4,128]{2,1,0:T(4,128)(2,1)S(1)} all-to-all(bf16[32,4,128]{2,1,0:T(4,128)(2,1)S(1)} %bitcast.21), channel_id=1, replica_groups=mesh['ep'=32,'y'=8,'x'=4] {'ep'}, dimensions={0} | all-to-all | bytes 65536 | tf_op jit(solution)/shard_map/all_to_all | solution.py:223
  95.9 0.3 shard_map.114
  96.2 11.8 %all_to_all.35.sq_ref = f32[32,1,128]{2,1,0:T(1,128)S(1)} all-to-all(f32[32,1,128]{2,1,0:T(1,128)S(1)} %get-tuple-element.24), channel_id=1, replica_groups=mesh['ep'=32,'y'=8,'x'=4] {'y','x'}, dimensions={0} | all-to-all | bytes 32768 | tf_op jit(solution)/shard_map/all_to_all | solution.py:223
  108.0 0.7 shard_map.115
Async XLA Ops:
  0.0 33.4 %copy-start = (bf16[2,128,1024]{2,1,0:T(8,128)(2,1)S(1)}, bf16[2,128,1024]{2,1,0:T(8,128)(2,1)}, u32[]{:S(2)}) copy-start(bf16[2,128,1024]{2,1,0:T(8,128)(2,1)} %wg_ref.1) | copy-start | bytes 1572868
  0.0 33.4 %copy-start.1 = (bf16[2,128,1024]{2,1,0:T(8,128)(2,1)S(1)}, bf16[2,128,1024]{2,1,0:T(8,128)(2,1)}, u32[]{:S(2)}) copy-start(bf16[2,128,1024]{2,1,0:T(8,128)(2,1)} %wu_ref.1) | copy-start | bytes 1572868
  0.0 33.4 %copy-start.3 = (bf16[128,1024]{1,0:T(8,128)(2,1)S(1)}, bf16[128,1024]{1,0:T(8,128)(2,1)}, u32[]{:S(2)}) copy-start(bf16[128,1024]{1,0:T(8,128)(2,1)} %sg_ref.1) | copy-start | bytes 786436
  0.0 33.4 %copy-start.4 = (bf16[128,1024]{1,0:T(8,128)(2,1)S(1)}, bf16[128,1024]{1,0:T(8,128)(2,1)}, u32[]{:S(2)}) copy-start(bf16[128,1024]{1,0:T(8,128)(2,1)} %su_ref.1) | copy-start | bytes 786436
  61.7 14.1 %copy-start.5 = (bf16[1024,128]{1,0:T(8,128)(2,1)S(1)}, bf16[1024,128]{1,0:T(8,128)(2,1)}, u32[]{:S(2)}) copy-start(bf16[1024,128]{1,0:T(8,128)(2,1)} %sd_ref.1) | copy-start | bytes 786436
  61.9 14.0 %copy-start.2 = (bf16[2,1024,128]{2,1,0:T(8,128)(2,1)S(1)}, bf16[2,1024,128]{2,1,0:T(8,128)(2,1)}, u32[]{:S(2)}) copy-start(bf16[2,1024,128]{2,1,0:T(8,128)(2,1)} %wd_ref.1) | copy-start | bytes 1572868

commit v6 on v5

--- a/solution.py
+++ b/solution.py
@@ -47,9 +47,9 @@
     return copies
 
 
-def dispatch_kernel(
+def load_kernel(
     routes_in, tokens_in, gates_in, gain_in, last_in,
-    out_ref, routes_ref, tokens_ref, gates_ref, gain_ref, last_ref, sems,
+    routes_ref, tokens_ref, gates_ref, gain_ref, last_ref, sems,
 ):
     copies = loads(
         (
@@ -61,12 +61,13 @@
         ),
         sems,
     )
-    copies[0].wait()
+    for c in copies:
+        c.wait()
+
+
+def route_kernel(routes_ref, tokens_ref, out_ref):
     choice = slot_choice(routes_ref[...])
-    copies[1].wait()
     out_ref[...] = dot(choice.astype(BF16), tokens_ref[...]).astype(BF16)
-    for c in copies[2:]:
-        c.wait()
 
 
 def row_of(col, lanes_from):
@@ -96,7 +97,6 @@
     shared_g = dot(toks_scaled, sg_ref[...])
     shared_u = dot(toks_scaled, su_ref[...])
     shared = jnp.where((iota((32, 1024), 0) & 7) < 4, shared_g, shared_u)
-    sub = iota((2, LANES), 0)
     for e in range(2):
         x = scaled[64 * e : 64 * e + 64]
         g = dot(x, wg_ref[e])
@@ -104,8 +104,7 @@
         for c in range(2):
             r = 2 * e + c
             sq = row_of(row_sq[32 * r : 32 * r + 32], 0) + row_of(tok_sq[8 * r : 8 * r + 8], 64)
-            hi = sq.astype(BF16).astype(F32)
-            sq2 = jnp.where(sub == 0, hi, sq - hi)
+            sq2 = halves(sq)
             for half in range(2):
                 blocks = []
                 for l in range(4 * half, 4 * half + 4):
@@ -120,12 +119,21 @@
                 out_ref[at : at + 4 * BLOCK, :] = jnp.concatenate(blocks, axis=0).astype(BF16)
 
 
+def halves(row):
+    hi = row.astype(BF16).astype(F32)
+    return jnp.where(iota((2, LANES), 0) == 0, hi, row - hi)
+
+
 def quarter_kernel(recv_ref, out_ref):
     n = out_ref.shape[0]
     total = recv_ref[0:n, :].astype(F32)
     for i in range(1, 4):
         total = total + recv_ref[n * i : n * i + n, :].astype(F32)
-    out_ref[...] = total.astype(BF16)
+    blocks = []
+    for q in range(n // BLOCK):
+        sq = BLOCK * q + BLOCK - 2
+        blocks += [total[BLOCK * q : sq], halves(total[sq : sq + 1] + total[sq + 1 : sq + 2])]
+    out_ref[...] = jnp.concatenate(blocks, axis=0).astype(BF16)
 
 
 def silu(v):
@@ -198,7 +206,7 @@
     out_ref[...] = (combined_ref[...] * scale * gain_ref[...].astype(F32)).astype(BF16)
 
 
-def call(kernel, out, fast, slow=()):
+def call(kernel, out, fast, slow=(), work=WORK):
     return pl.pallas_call(
         kernel,
         out_shape=out,
@@ -206,7 +214,7 @@
         + [pl.BlockSpec(memory_space=pltpu.HBM)] * len(slow),
         scratch_shapes=[pltpu.SemaphoreType.DMA((len(slow),))] if slow else [],
         compiler_params=pltpu.CompilerParams(vmem_limit_bytes=16 << 20),
-        cost_estimate=pl.CostEstimate(flops=WORK, bytes_accessed=1 << 16, transcendentals=0),
+        cost_estimate=pl.CostEstimate(flops=work, bytes_accessed=1 << 16, transcendentals=0),
     )(*[pltpu.with_memory_space_constraint(a, pltpu.VMEM) for a in fast], *[pltpu.with_memory_space_constraint(a, pltpu.HBM) for a in slow])
 
 
@@ -243,9 +251,10 @@
         pre_gain.reshape(1, LANES),
         out_gain.reshape(1, LANES),
     )
-    outgoing, routes, tokens, gates, gain, out_gain = call(
-        dispatch_kernel, (fast((ROWS, LANES), BF16), *[like(a) for a in first]), (), first
-    )
+    routes, tokens, gates, gain, out_gain = call(
+        load_kernel, tuple(like(a) for a in first), (), first, 1
+    )
+    outgoing = call(route_kernel, fast((ROWS, LANES), BF16), (routes, tokens))
     received = swapped(outgoing, "ep", 4)
     weights = (expert_gate, expert_up, shared_gate, shared_up)
     partial = call(

time: 109 us -> 109 us (level)
    pallas_call x7 -> x8, Pallas kernels: 3.19 us -> 3.1 us  [call(): pl.pallas_call(kernel, out_shape=out, in_specs=[pl.BlockSpec(memory_space...]
where the time goes in v6:
time: 109 us
  blocking collectives  106 us (97%)
  Pallas kernels  3.1 us (3%)
    all_to_all x6, blocking collectives, swapped(): return lax.all_to_all(tiles, axis, 0, 0, tiled=True).reshape(x.shape)  106 us
    pallas_call x8, Pallas kernels, call(): pl.pallas_call(kernel, out_shape=out, in_specs=[pl.BlockSpec(memory_space...  3.1 us

profile of v6, /device:TPU:1, one launch (start us, length us, event | category | flops | bytes accessed | tf_op | source)
XLA Modules:
  0.0 108.8 jit_solution(9509175590357020767)
XLA Ops:
  0.0 0.8 shard_map.109
  0.8 0.0 copy-start
  0.8 0.0 copy-start.1
  0.8 0.0 copy-start.3
  0.8 0.0 copy-start.4
  0.8 0.3 shard_map.110
  1.1 32.4 %all_to_all.30 = bf16[32,4,128]{2,1,0:T(4,128)(2,1)S(1)} all-to-all(bf16[32,4,128]{2,1,0:T(4,128)(2,1)S(1)} %bitcast.23), channel_id=1, replica_groups=mesh['ep'=32,'y'=8,'x'=4] {'ep'}, dimensions={0} | all-to-all | bytes 65536 | tf_op jit(solution)/shard_map/all_to_all | solution.py:231
  33.5 0.0 copy-done
  33.5 0.0 copy-done.1
  33.5 0.0 copy-done.3
  33.5 0.0 copy-done.4
  33.5 0.5 shard_map.111
  34.0 12.8 %all_to_all.31 = bf16[1184,2,128]{2,1,0:T(2,128)(2,1)S(1)} all-to-all(bf16[1184,2,128]{2,1,0:T(2,128)(2,1)S(1)} %bitcast.14), channel_id=1, replica_groups=mesh['ep'=32,'y'=8,'x'=4] {'x'}, dimensions={0} | all-to-all | bytes 1212416 | tf_op jit(solution)/shard_map/all_to_all | solution.py:231
  46.8 0.1 shard_map.112
  46.9 14.9 %all_to_all.32 = bf16[296,2,128]{2,1,0:T(2,128)(2,1)S(1)} all-to-all(bf16[296,2,128]{2,1,0:T(2,128)(2,1)S(1)} %bitcast.18), channel_id=1, replica_groups=mesh['ep'=32,'y'=8,'x'=4] {'y'}, dimensions={0} | all-to-all | bytes 303104 | tf_op jit(solution)/shard_map/all_to_all | solution.py:231
  61.8 0.0 copy-start.5
  61.8 0.1 shard_map.113
  61.9 0.0 copy-start.2
  61.9 14.0 %all_to_all.33 = bf16[288,4,128]{2,1,0:T(4,128)(2,1)S(1)} all-to-all(bf16[288,4,128]{2,1,0:T(4,128)(2,1)S(1)} %bitcast.17), channel_id=1, replica_groups=mesh['ep'=32,'y'=8,'x'=4] {'y','x'}, dimensions={0} | all-to-all | bytes 589824 | tf_op jit(solution)/shard_map/all_to_all | solution.py:231
  75.9 0.0 copy-done.5
  75.9 0.0 copy-done.2
  75.9 0.4 shard_map.114
  76.3 19.4 %all_to_all.34 = bf16[32,4,128]{2,1,0:T(4,128)(2,1)S(1)} all-to-all(bf16[32,4,128]{2,1,0:T(4,128)(2,1)S(1)} %bitcast.20), channel_id=1, replica_groups=mesh['ep'=32,'y'=8,'x'=4] {'ep'}, dimensions={0} | all-to-all | bytes 65536 | tf_op jit(solution)/shard_map/all_to_all | solution.py:231
  95.7 0.3 shard_map.115
  96.0 12.0 %all_to_all.35.sq_ref = f32[32,1,128]{2,1,0:T(1,128)S(1)} all-to-all(f32[32,1,128]{2,1,0:T(1,128)S(1)} %get-tuple-element.22), channel_id=1, replica_groups=mesh['ep'=32,'y'=8,'x'=4] {'y','x'}, dimensions={0} | all-to-all | bytes 32768 | tf_op jit(solution)/shard_map/all_to_all | solution.py:231
  108.0 0.7 shard_map.116
Async XLA Ops:
  0.8 32.7 %copy-start = (bf16[2,128,1024]{2,1,0:T(8,128)(2,1)S(1)}, bf16[2,128,1024]{2,1,0:T(8,128)(2,1)}, u32[]{:S(2)}) copy-start(bf16[2,128,1024]{2,1,0:T(8,128)(2,1)} %wg_ref.1) | copy-start | bytes 1572868
  0.8 32.7 %copy-start.1 = (bf16[2,128,1024]{2,1,0:T(8,128)(2,1)S(1)}, bf16[2,128,1024]{2,1,0:T(8,128)(2,1)}, u32[]{:S(2)}) copy-start(bf16[2,128,1024]{2,1,0:T(8,128)(2,1)} %wu_ref.1) | copy-start | bytes 1572868
  0.8 32.7 %copy-start.3 = (bf16[128,1024]{1,0:T(8,128)(2,1)S(1)}, bf16[128,1024]{1,0:T(8,128)(2,1)}, u32[]{:S(2)}) copy-start(bf16[128,1024]{1,0:T(8,128)(2,1)} %sg_ref.1) | copy-start | bytes 786436
  0.8 32.7 %copy-start.4 = (bf16[128,1024]{1,0:T(8,128)(2,1)S(1)}, bf16[128,1024]{1,0:T(8,128)(2,1)}, u32[]{:S(2)}) copy-start(bf16[128,1024]{1,0:T(8,128)(2,1)} %su_ref.1) | copy-start | bytes 786436
  61.8 14.1 %copy-start.5 = (bf16[1024,128]{1,0:T(8,128)(2,1)S(1)}, bf16[1024,128]{1,0:T(8,128)(2,1)}, u32[]{:S(2)}) copy-start(bf16[1024,128]{1,0:T(8,128)(2,1)} %sd_ref.1) | copy-start | bytes 786436
  61.9 14.0 %copy-start.2 = (bf16[2,1024,128]{2,1,0:T(8,128)(2,1)S(1)}, bf16[2,1024,128]{2,1,0:T(8,128)(2,1)}, u32[]{:S(2)}) copy-start(bf16[2,1024,128]{2,1,0:T(8,128)(2,1)} %wd_ref.1) | copy-start | bytes 1572868
